TPU v7x, 256 devices: a whole 4x4x8 slice. The times are simulated.
256 devices in a mesh: ep: 64 (over z, x, core), tp: 4 (over y).
Axes of the slice: x: 4, y: 4, z: 8, core: 2. Of those that a mesh axis runs over, the one named last changes fastest.
Arguments:
- pool_input: bfloat16 [32768, 1024], P('ep', 'tp'), may hold values from -6 to 6
- group_weight: bfloat16 [4, 256, 256], P('tp'), may hold values from -0.375 to 0.375
- pool_scale: float32 [1024], P('tp'), may hold values from 0.1 to 1.9
- out_weight: bfloat16 [1024, 2048], P('tp'), may hold values from -0.1875 to 0.1875
- mix_gain: float32 [2048], replicated, may hold values from 0.1 to 1.9
- expert_input: bfloat16 [65536, 2048], P(('ep', 'tp')), may hold values from -6 to 6
- routes: int32 [65536, 2], P('ep'), may hold values from 0 to 127, all different within a row; in each aligned block of 256 rows (0 to 255, 256 to 511, ...) at most 5 rows name the same one
- route_weights: float32 [65536, 2], P('ep'), may hold values from 0.2 to 2.5
- moe_in_gain: float32 [2048], replicated, may hold values from 0.1 to 1.9
- gate_weight: bfloat16 [128, 2048, 1024], P('ep', None, 'tp'), may hold values from -0.125 to 0.125
- up_weight: bfloat16 [128, 2048, 1024], P('ep', None, 'tp'), may hold values from -0.125 to 0.125
- down_weight: bfloat16 [128, 1024, 2048], P('ep', 'tp'), may hold values from -0.1875 to 0.1875
- moe_out_gain: float32 [2048], replicated, may hold values from 0.1 to 1.9
Outputs:
- mixer_out: bfloat16 [32768, 2048], P(('ep', 'tp'))
- moe_out: bfloat16 [65536, 2048], P(('ep', 'tp'))
Inputs may be any that keep to these rules, and one draw needn't show every extreme that they name: `routes`: each row names 2 different experts. In each aligned block of 256 rows no expert is named by more than 5 rows, a bound that some block reaches.
All inputs are finite; a program needn't handle non-finite values.
Results may differ from a plain program's by a relative error of at most 0.013.
Values may be sent and summed in bfloat16 or wider, within the bound.
No kernel may reach another device: no remote copies, remote signals or barrier semaphores. Data moves between devices by JAX's collectives and lax.ppermute only.
A program may use at most 128 MiB of HBM per device.

v0:
```python
import jax
import jax.numpy as jnp
from jax import lax
from jax.sharding import PartitionSpec as P

NORM_EPS = 1e-06


def passed_along(value, axis, steps):
    count = lax.axis_size(axis)
    initial, last = (max(0, -steps), min(count, count - steps))
    return lax.ppermute(value, axis, [(source, source + steps) for source in range(initial, last)])


def rms_scale(values, gain_vec):
    mean_sq = jnp.mean(values * values, axis=-1, keepdims=True)
    return values * lax.rsqrt(mean_sq + NORM_EPS) * gain_vec


def slot_numbers(route_block, experts, capacity):
    flat_routes = route_block.reshape(-1)
    one_hot = (flat_routes[:, None] == jnp.arange(experts, dtype=jnp.int32)[None, :]).astype(
        jnp.int32
    )
    slot_rank = jnp.sum((jnp.cumsum(one_hot, axis=0) - one_hot) * one_hot, axis=1)
    return flat_routes * capacity + slot_rank


def fill_table(slot_ids, payload, empty_value, slots_total):
    return jnp.full((slots_total,), empty_value, payload.dtype).at[slot_ids].set(payload)


def on_device(
    pool_input,
    group_weight,
    pool_scale,
    out_weight,
    mix_gain,
    expert_input,
    routes,
    route_weights,
    moe_in_gain,
    gate_weight,
    up_weight,
    down_weight,
    moe_out_gain,
):
    tp_size = lax.axis_size("tp")
    ep_size = lax.axis_size("ep")
    tp_index = lax.axis_index("tp")
    rows_a = pool_input.shape[0]
    model_width = out_weight.shape[1]
    history_rows = 2**tp_size
    window = jnp.left_shift(jnp.int32(2), tp_index)
    history = passed_along(pool_input[rows_a - history_rows :], "ep", 1)
    extended = jnp.concatenate([history, pool_input], axis=0).astype(jnp.float32)
    running = jnp.cumsum(extended, axis=0)
    lagged = lax.dynamic_slice_in_dim(running, history_rows - window, rows_a, 0)
    current = running[history_rows:]
    position = lax.axis_index("ep") * rows_a + jnp.arange(rows_a, dtype=jnp.int32)
    divisor = jnp.minimum(position + 1, window).astype(jnp.float32)[:, None]
    pooled = ((current - lagged) / divisor - extended[history_rows:]).astype(jnp.bfloat16)
    grouped = (
        jnp.dot(pooled, group_weight[0], preferred_element_type=jnp.float32) * pool_scale
    ).astype(jnp.bfloat16)
    exp_dev = gate_weight.shape[0]
    experts = exp_dev * ep_size
    tok_dev = expert_input.shape[0]
    top_count = routes.shape[1]
    capacity = max(2, 5 * tok_dev * top_count // (4 * experts))
    slots_total = experts * capacity
    normed = rms_scale(expert_input.astype(jnp.float32), moe_in_gain).astype(jnp.bfloat16)
    own_routes = lax.dynamic_slice_in_dim(routes, tp_index * tok_dev, tok_dev, 0)
    own_slots = slot_numbers(own_routes, experts, capacity)
    pair_token = jnp.arange(tok_dev * top_count, dtype=jnp.int32) // top_count
    token_table = fill_table(own_slots, pair_token, tok_dev, slots_total)
    padded_rows = jnp.concatenate([normed, jnp.zeros((1, model_width), jnp.bfloat16)], axis=0)
    outgoing = padded_rows[token_table].reshape(ep_size, exp_dev * capacity, model_width)
    arrived = lax.all_to_all(outgoing, "ep", split_axis=0, concat_axis=0, tiled=True)
    received = lax.all_gather(arrived[None], "tp", axis=0, tiled=True)
    per_quarter = ep_size * exp_dev * capacity
    flat_in = received.reshape(tp_size * per_quarter, model_width)
    projected = lax.psum_scatter(
        jnp.dot(grouped, out_weight, preferred_element_type=jnp.float32).astype(jnp.bfloat16),
        "tp",
        scatter_dimension=0,
        tiled=True,
    ).astype(jnp.float32)
    piece_rows = flat_in
    piece_rows = piece_rows.reshape(
        per_quarter * lax.axis_size("tp") // (exp_dev * capacity), exp_dev, capacity, model_width
    )
    gate_act = jnp.einsum(
        "nxcd,xdf->nxcf", piece_rows, gate_weight, preferred_element_type=jnp.float32
    )
    up_act = jnp.einsum("nxcd,xdf->nxcf", piece_rows, up_weight, preferred_element_type=jnp.float32)
    hidden = (jax.nn.silu(gate_act) * up_act).astype(jnp.bfloat16)
    down_act = jnp.einsum("nxcf,xfd->nxcd", hidden, down_weight, preferred_element_type=jnp.float32)
    expert_sum = lax.psum_scatter(
        down_act.reshape(per_quarter * lax.axis_size("tp"), model_width).astype(jnp.bfloat16),
        "tp",
        scatter_dimension=0,
        tiled=True,
    )
    mixer_out = rms_scale(projected, mix_gain).astype(jnp.bfloat16)
    expert_back = expert_sum.reshape(ep_size, exp_dev * capacity, model_width)
    returned = lax.all_to_all(expert_back, "ep", split_axis=0, concat_axis=0, tiled=True)
    picked = returned.reshape(slots_total, model_width)[own_slots].reshape(
        tok_dev, top_count, model_width
    )
    own_weights = lax.dynamic_slice_in_dim(route_weights, tp_index * tok_dev, tok_dev, 0)
    combined = jnp.sum(picked.astype(jnp.float32) * own_weights[:, :, None], axis=1)
    moe_out = rms_scale(combined, moe_out_gain).astype(jnp.bfloat16)
    return (mixer_out, moe_out)


def solution(mesh):
    in_specs = (
        P("ep", "tp"),
        P("tp", None, None),
        P("tp"),
        P("tp", None),
        P(),
        P(("ep", "tp"), None),
        P("ep", None),
        P("ep", None),
        P(),
        P("ep", None, "tp"),
        P("ep", None, "tp"),
        P("ep", "tp", None),
        P(),
    )
    out_specs = (P(("ep", "tp"), None), P(("ep", "tp"), None))
    return jax.shard_map(
        on_device, mesh=mesh, in_specs=in_specs, out_specs=out_specs, check_vma=False
    )
```

profile of v0, /device:TPU:2, one launch (start us, length us, event | category | flops | bytes accessed | tf_op | source)
XLA Modules:
  0.0 536.5 jit_solution(6434303387397360393)
XLA Ops:
  7.2 0.0 copy-start
  7.2 0.0 copy-start.2
  7.2 0.0 copy-start.6
  7.2 0.0 all-gather.3.cloned.1.call-start
  7.3 0.8 broadcast_multiply_fusion
  8.1 0.1 copy.31
  8.2 0.1 eq.29
  8.4 0.1 eq.25
  8.5 0.6 add_select_fusion
  9.1 0.1 copy.33
  9.2 0.2 fusion.29
  9.5 0.1 copy.30
  9.7 0.1 mul.122
  9.8 0.2 fusion.28
  10.1 2.6 scatter_custom_fusion
  12.7 0.0 copy-done.2
  12.7 0.3 fusion.4
  13.0 0.0 copy-done.6
  13.0 0.3 fusion.6
  13.3 0.1 concatenate.7
  13.4 4.1 gather_fusion
  17.5 5.4 %reshape.113 = bf16[64,10,2048]{2,1,0:T(8,128)(2,1)} reshape(bf16[640,2048]{1,0:T(8,128)(2,1)} %gather_fusion) | data formatting | bytes 5242880 | tf_op jit(solution)/shard_map/reshape | solution.py:78
  22.9 108.2 %all_to_all.10 = bf16[64,10,2048]{2,1,0:T(8,128)(2,1)S(1)} all-to-all(bf16[64,10,2048]{2,1,0:T(8,128)(2,1)} %reshape.113), channel_id=1, replica_groups=mesh['ep'=64,'tp'=4] {'ep'}, dimensions={0} | all-to-all | bytes 5242880 | tf_op jit(solution)/shard_map/all_to_all | solution.py:79
  131.1 3.0 copy.35
  134.0 0.0 all-gather.3.cloned.1.call-update
  134.1 0.2 reduce-scatter.5.cloned.1.call-start
  134.3 99.6 %all-gather.3.cloned.1.call-done = bf16[256,10,2048]{2,0,1:T(8,128)(2,1)} async-done(((bf16[64,10,2048]{2,0,1:T(8,128)(2,1)}), bf16[256,10,2048]{2,0,1:T(8,128)(2,1)}) %all-gather.3.cloned.1.call-update) | async-done | bytes 10485776 | tf_op jit(solution)/shard_map/all_gather | solution.py:80
  233.9 9.0 %fusion.14 = f32[2,256,5,256]{3,1,2,0:T(8,128)} fusion(bf16[256,2,5,2048]{3,0,2,1:T(8,128)(2,1)} %bitcast.84, bf16[2,2048,256]{2,1,0:T(8,128)(2,1)} %param.22), kind=kOutput, calls=%fused_computation.21 | convolution fusion | flops 2684354560 | bytes 15204352 | tf_op jit(solution)/shard_map/nxcd,xdf->nxcf/dot_general | solution.py:93
  242.9 0.0 copy-done
  242.9 16.3 %convert_bitcast_fusion = bf16[256,2,5,2048]{3,0,2,1:T(8,128)(2,1)} fusion(bf16[2,256,2048]{2,1,0:T(8,128)(2,1)S(1)} %copy-done, f32[2,256,5,256]{3,1,2,0:T(8,128)} %fusion.14, bf16[256,2,5,2048]{3,0,2,1:T(8,128)(2,1)} %bitcast.85, bf16[2,2048,256]{2,1,0:T(8,128)(2,1)} %param.23), kind=kOutput, calls=%fused_computation.3 | convolution fusion | flops 5377884160 | bytes 27787264 | tf_op jit(solution)/shard_map/nxcf,xfd->nxcd/dot_general | solution.py:98
  259.2 15.3 %copy.36 = bf16[256,2,5,2048]{3,2,1,0:T(8,128)(2,1)} copy(bf16[256,2,5,2048]{3,0,2,1:T(8,128)(2,1)} %convert_bitcast_fusion) | data formatting | bytes 20971520 | tf_op jit(solution)/shard_map/convert_element_type | solution.py:100
  274.5 18.4 %convert_element_type.73 = bf16[2560,2048]{1,0:T(8,128)(2,1)} reshape(bf16[256,2,5,2048]{3,2,1,0:T(8,128)(2,1)} %copy.36) | data formatting | bytes 20971520 | tf_op jit(solution)/shard_map/convert_element_type | solution.py:100
  293.0 0.0 reduce-scatter.5.cloned.1.call-update
  293.0 0.9 copy-done.4
  293.9 1.9 collective-permute-start
  295.9 3.0 collective-permute-done
  298.9 0.1 fusion.37
  299.0 0.7 fusion.21
  299.7 0.1 broadcast_add_fusion
  299.8 0.2 copy.29
  300.0 94.2 %reduce-scatter.5.cloned.1.call-done = bf16[640,2048]{1,0:T(8,128)(2,1)} async-done(((bf16[2560,2048]{1,0:T(8,128)(2,1)}), bf16[640,2048]{1,0:T(8,128)(2,1)}) %reduce-scatter.5.cloned.1.call-update) | async-done | bytes 2621456 | tf_op jit(solution)/shard_map/reduce_scatter | solution.py:99
  394.2 5.4 %reshape.114 = bf16[64,10,2048]{2,1,0:T(8,128)(2,1)} reshape(bf16[640,2048]{1,0:T(8,128)(2,1)} %reduce-scatter.5.cloned.1.call-done) | data formatting | bytes 5242880 | tf_op jit(solution)/shard_map/reshape | solution.py:106
  399.6 10.9 %all-to-all-start.1 = ((bf16[64,10,2048]{2,1,0:T(8,128)(2,1)}), bf16[64,10,2048]{2,1,0:T(8,128)(2,1)}, u32[]{:S(2)}, u32[]{:S(2)}) async-start(bf16[64,10,2048]{2,1,0:T(8,128)(2,1)} %reshape.114), calls=%async_computation.3 | async-start | bytes 8388608 | tf_op jit(solution)/shard_map/all_to_all | solution.py:107
  410.5 0.3 reduce-scatter.3.cloned.1.call-start
  410.8 0.0 copy-done.3
  410.8 0.0 copy-done.5
  410.8 0.0 copy-done.9
  410.8 0.0 copy-start.7
  410.8 2.3 convolution_convert_fusion
  413.1 0.0 reduce-scatter.3.cloned.1.call-update
  413.1 0.7 constant_dynamic-slice_fusion
  413.8 0.1 copy.37
  414.0 31.7 %reduce-scatter.3.cloned.1.call-done = bf16[128,2048]{1,0:T(8,128)(2,1)} async-done(((bf16[512,2048]{1,0:T(8,128)(2,1)}), bf16[128,2048]{1,0:T(8,128)(2,1)}) %reduce-scatter.3.cloned.1.call-update) | async-done | bytes 524304 | tf_op jit(solution)/shard_map/reduce_scatter | solution.py:83
  445.6 1.2 fusion.18
  446.9 0.0 copy-done.7
  446.9 2.0 fusion.20
  448.9 57.7 %all-to-all-done.1 = bf16[64,10,2048]{2,1,0:T(8,128)(2,1)} async-done(((bf16[64,10,2048]{2,1,0:T(8,128)(2,1)}), bf16[64,10,2048]{2,1,0:T(8,128)(2,1)}, u32[]{:S(2)}, u32[]{:S(2)}) %all-to-all-start.1) | async-done | bytes 2621472 | tf_op jit(solution)/shard_map/all_to_all | solution.py:107
  506.6 4.1 reshape.115
  510.7 3.3 gather_fusion.1
  514.0 5.4 %reshape.116 = f32[256,2,2048]{2,1,0:T(2,128)} reshape(bf16[512,2048]{1,0:T(8,128)(2,1)} %gather_fusion.1) | data formatting | bytes 6291456 | tf_op jit(solution)/shard_map/convert_element_type | solution.py:112
  519.5 9.0 %multiply_reduce_fusion = f32[256,2048]{1,0:T(8,128)S(1)} fusion(f32[256,2,2048]{2,1,0:T(2,128)} %reshape.116, f32[256,2]{1,0:T(8,128)S(1)} %copy.37), kind=kLoop, calls=%fused_computation.4 | loop fusion | flops 1572864 | bytes 6293504 | tf_op jit(solution)/shard_map/reduce_sum | solution.py:112
  528.5 0.2 multiply_reduce_fusion.1
  528.7 0.0 copy-done.8
  528.7 1.2 multiply_convert_fusion
  (26 shorter events, 0.3 us)
Async XLA Ops:
  7.2 235.7 %copy-start = (bf16[2,256,2048]{2,1,0:T(8,128)(2,1)S(1)}, bf16[2,256,2048]{2,1,0:T(8,128)(2,1)}, u32[]{:S(2)}) copy-start(bf16[2,256,2048]{2,1,0:T(8,128)(2,1)} %param.24) | copy-start | bytes 6291460
  7.2 5.5 %copy-start.2 = (bf16[256,2048]{1,0:T(8,128)(2,1)S(1)}, bf16[256,2048]{1,0:T(8,128)(2,1)}, u32[]{:S(2)}) copy-start(bf16[256,2048]{1,0:T(8,128)(2,1)} %param.18) | copy-start | bytes 3145732
  7.2 5.8 %copy-start.6 = (f32[2048]{0:T(1024)S(1)}, f32[2048]{0:T(1024)}, u32[]{:S(2)}) copy-start(f32[2048]{0:T(1024)} %param.21) | copy-start | bytes 24580
  7.2 226.7 %all-gather.3.cloned.1.call-start = ((), (), s32[]{:S(2)}) async-start(), calls=%async_computation.6 | async-start | bytes 13107200 | tf_op jit(solution)/shard_map/all_gather | solution.py:80
  134.1 260.2 %reduce-scatter.5.cloned.1.call-start = ((), (), s32[]{:S(2)}) async-start(), calls=%async_computation.5 | async-start | bytes 13107200 | tf_op jit(solution)/shard_map/reduce_scatter | solution.py:99
  293.0 0.9 copy-start.4
  293.9 5.0 collective-permute-start
  399.6 11.2 %copy-start.3 = (bf16[256,2048]{1,0:T(8,128)(2,1)S(1)}, bf16[256,2048]{1,0:T(8,128)(2,1)}, u32[]{:S(2)}) copy-start(bf16[256,2048]{1,0:T(8,128)(2,1)} %param.16) | copy-start | bytes 3145732
  399.6 11.2 %copy-start.5 = (bf16[1,256,256]{2,1,0:T(8,128)(2,1)S(1)}, bf16[1,256,256]{2,1,0:T(8,128)(2,1)}, u32[]{:S(2)}) copy-start(bf16[1,256,256]{2,1,0:T(8,128)(2,1)} %param.14) | copy-start | bytes 393220
  399.6 11.2 %copy-start.9 = (f32[256]{0:T(256)S(1)}, f32[256]{0:T(256)}, u32[]{:S(2)}) copy-start(f32[256]{0:T(256)} %param.15) | copy-start | bytes 3076
  399.6 107.0 %all-to-all-start.1 = ((bf16[64,10,2048]{2,1,0:T(8,128)(2,1)}), bf16[64,10,2048]{2,1,0:T(8,128)(2,1)}, u32[]{:S(2)}, u32[]{:S(2)}) async-start(bf16[64,10,2048]{2,1,0:T(8,128)(2,1)} %reshape.114), calls=%async_computation.3 | async-start | bytes 8388608 | tf_op jit(solution)/shard_map/all_to_all | solution.py:107
  410.5 35.1 %reduce-scatter.3.cloned.1.call-start = ((), (), s32[]{:S(2)}) async-start(), calls=%async_computation.4 | async-start | bytes 2621440 | tf_op jit(solution)/shard_map/reduce_scatter | solution.py:83
  410.8 36.1 %copy-start.7 = (f32[2048]{0:T(1024)S(1)}, f32[2048]{0:T(1024)}, u32[]{:S(2)}) copy-start(f32[2048]{0:T(1024)} %param.17) | copy-start | bytes 24580
  519.4 9.3 %copy-start.8 = (f32[2048]{0:T(1024)S(1)}, f32[2048]{0:T(1024)}, u32[]{:S(2)}) copy-start(f32[2048]{0:T(1024)} %param.25) | copy-start | bytes 24580
  519.4 10.5 %copy-start.1 = (bf16[2,256,2048]{2,1,0:T(8,128)(2,1)S(1)}, bf16[2,256,2048]{2,1,0:T(8,128)(2,1)}, u32[]{:S(2)}) copy-start(bf16[2,256,2048]{2,1,0:T(8,128)(2,1)} %param.24) | copy-start | bytes 6291460
Sparse Core Ops, SparseCore 0:
  134.2 99.7 all-gather.2
  293.1 101.0 reduce-scatter.4
  413.9 31.7 reduce-scatter.2
where the time goes:
time: 538 us; the launch traced here: 536 us
  waiting for transfers between devices  286 us (53%)
  blocking collectives  108 us (20%)
  local copies, waits for them, and re-layouts  70 us (13%)
  matrix products  27.6 us (5%)
  other arithmetic  17.1 us (3%)
  between operations  14.1 us (3%)
  starting transfers between devices  13.3 us (2%)
    all_to_all x1, blocking collectives, on_device(): lax.all_to_all(outgoing, 'ep', split_axis=0, concat_axis=0, tiled=True)  108 us
    all_gather x1, waiting for transfers between devices, on_device(): received = lax.all_gather(arrived[None], 'tp', axis=0, tiled=True)  99.6 us
    reduce_scatter x1, waiting for transfers between devices, on_device(): lax.psum_scatter(down_act.reshape(per_quarter * lax.axis_size('tp'), mode...  94.2 us
    all_to_all x1, waiting for transfers between devices, on_device(): lax.all_to_all(expert_back, 'ep', split_axis=0, concat_axis=0, tiled=True)  57.7 us
    convert_element_type x2, local copies, waits for them, and re-layouts, on_device(): down_act.reshape(per_quarter * lax.axis_size('tp'), model_width)  33.8 us
    reduce_scatter x1, waiting for transfers between devices, on_device(): lax.psum_scatter(jnp.dot(grouped, out_weight, preferred_element_type=jnp....  31.7 us
    dot_general x1, matrix products, on_device(): jnp.einsum('nxcf,xfd->nxcd', hidden, down_weight, preferred_element_type=...  16.3 us
    all_to_all x1, starting transfers between devices, on_device(): lax.all_to_all(expert_back, 'ep', split_axis=0, concat_axis=0, tiled=True)  10.9 us
  transfers between devices with their start and end apart: 5, of which 5 were waited for; matrix products, arithmetic and copies ran while one was open for 1% of the time, Pallas kernels for 0%

commit v1 on v0

--- a/solution.py
+++ b/solution.py
@@ -1,9 +1,29 @@
+import functools
 import jax
 import jax.numpy as jnp
 from jax import lax
 from jax.sharding import PartitionSpec as P
 
 NORM_EPS = 1e-06
+
+
+def take_stacks_all(u_in, row_axis):
+    block_out, t1, z2 = (lax.axis_size(row_axis), lax.axis_index(row_axis), u_in.shape[0])
+    cards = [d * block_out if s == 0 else d for s, d in enumerate(u_in.shape)]
+    z1 = lax.dynamic_update_slice_in_dim(jnp.zeros(cards, u_in.dtype), u_in, t1 * z2, axis=0)
+    y_new = a_now = u_in
+    for tick in range(1, block_out // 2 + 1):
+        y_new = lax.ppermute(y_new, row_axis, [(s, (s + 1) % block_out) for s in range(block_out)])
+        z1 = lax.dynamic_update_slice_in_dim(z1, y_new, (t1 - tick) % block_out * z2, axis=0)
+        if 2 * tick < block_out:
+            a_now = lax.ppermute(
+                a_now, row_axis, [(s, (s - 1) % block_out) for s in range(block_out)]
+            )
+            z1 = lax.dynamic_update_slice_in_dim(z1, a_now, (t1 + tick) % block_out * z2, axis=0)
+    return z1
+
+
+take_edges = functools.partial(take_stacks_all, row_axis="tp")
 
 
 def passed_along(value, axis, steps):
@@ -77,7 +97,7 @@
     padded_rows = jnp.concatenate([normed, jnp.zeros((1, model_width), jnp.bfloat16)], axis=0)
     outgoing = padded_rows[token_table].reshape(ep_size, exp_dev * capacity, model_width)
     arrived = lax.all_to_all(outgoing, "ep", split_axis=0, concat_axis=0, tiled=True)
-    received = lax.all_gather(arrived[None], "tp", axis=0, tiled=True)
+    received = take_edges(arrived[None])
     per_quarter = ep_size * exp_dev * capacity
     flat_in = received.reshape(tp_size * per_quarter, model_width)
     projected = lax.psum_scatter(

time: 538 us -> 555 us (1.032)
  local copies, waits for them, and re-layouts: 70 us -> 89 us
    all_gather x1 -> x0, waiting for transfers between devices: 99.6 us -> none  [on_device(): received = lax.all_gather(arrived[None], 'tp', axis=0, tiled=True)]
    ppermute x0 -> x3, waiting for transfers between devices: none -> 97.6 us  [the longest x2 97.6 us: take_stacks_all(): lax.ppermute(y_new, row_axis, [(s, (s + 1) % block_out) for s in range(bl...]
    dynamic_update_slice x0 -> x4, local copies, waits for them, and re-layouts: none -> 13.6 us  [the longest x2 7.15 us: take_stacks_all(): lax.dynamic_update_slice_in_dim(z1, y_new, (t1 - tick) % block_out * z2,...]
    broadcast_in_dim x0 -> x2, local copies, waits for them, and re-layouts: none -> 8.29 us  [the longest x1 5.32 us: take_stacks_all(): jnp.zeros(cards, u_in.dtype)]
  transfers between devices with their start and end apart: 5 -> 7, of which waited for: 5 -> 6; matrix products, arithmetic and copies ran while one was open for 1% -> 4% of each run, Pallas kernels for 0% -> 0%
where the time goes in v1:
time: 555 us; the launch traced here: 553 us
  waiting for transfers between devices  281 us (51%)
  blocking collectives  108 us (19%)
  local copies, waits for them, and re-layouts  89 us (16%)
  matrix products  27 us (5%)
  other arithmetic  17.1 us (3%)
  starting transfers between devices  16.6 us (3%)
  between operations  14.4 us (3%)
    all_to_all x1, blocking collectives, on_device(): lax.all_to_all(outgoing, 'ep', split_axis=0, concat_axis=0, tiled=True)  108 us
    ppermute x2, waiting for transfers between devices, take_stacks_all(): lax.ppermute(y_new, row_axis, [(s, (s + 1) % block_out) for s in range(bl...  97.6 us
    reduce_scatter x1, waiting for transfers between devices, on_device(): lax.psum_scatter(down_act.reshape(per_quarter * lax.axis_size('tp'), mode...  90.7 us
    all_to_all x1, waiting for transfers between devices, on_device(): lax.all_to_all(expert_back, 'ep', split_axis=0, concat_axis=0, tiled=True)  57.7 us
    convert_element_type x2, local copies, waits for them, and re-layouts, on_device(): down_act.reshape(per_quarter * lax.axis_size('tp'), model_width)  33.8 us
    reduce_scatter x1, waiting for transfers between devices, on_device(): lax.psum_scatter(jnp.dot(grouped, out_weight, preferred_element_type=jnp....  31.9 us
    dot_general x1, matrix products, on_device(): jnp.einsum('nxcf,xfd->nxcd', hidden, down_weight, preferred_element_type=...  16.3 us
  transfers between devices with their start and end apart: 7, of which 6 were waited for; matrix products, arithmetic and copies ran while one was open for 4% of the time, Pallas kernels for 0%

profile of v1, /device:TPU:2, one launch (start us, length us, event | category | flops | bytes accessed | tf_op | source)
XLA Modules:
  0.0 552.9 jit_solution(3545508925043076282)
XLA Ops:
  7.2 0.0 copy-start
  7.2 0.0 reduce-scatter.5.cloned.1.call-start
  7.3 0.8 broadcast_multiply_fusion
  8.1 0.1 copy.37
  8.2 0.1 eq.33
  8.4 0.1 eq.29
  8.5 0.6 add_select_fusion
  9.1 0.1 copy.39
  9.2 0.2 fusion.29
  9.5 0.1 copy.36
  9.7 0.1 mul.122
  9.8 0.2 fusion.28
  10.1 2.6 scatter_custom_fusion
  12.7 0.0 copy-done.4
  12.7 0.3 fusion.4
  13.0 0.3 fusion.6
  13.3 0.1 concatenate.7
  13.4 4.1 gather_fusion
  17.5 5.4 reshape.113
  22.9 108.2 %all_to_all.10 = bf16[64,10,2048]{2,1,0:T(8,128)(2,1)S(1)} all-to-all(bf16[64,10,2048]{2,1,0:T(8,128)(2,1)} %reshape.113), channel_id=1, replica_groups=mesh['ep'=64,'tp'=4] {'ep'}, dimensions={0} | all-to-all | bytes 5242880 | tf_op jit(solution)/shard_map/all_to_all | solution.py:99
  131.1 3.0 copy.42
  134.1 0.0 copy-done.2
  134.1 1.6 collective-permute-start.1
  135.6 1.7 collective-permute-start.2
  137.3 55.4 %collective-permute-done.1 = bf16[1,64,10,2048]{3,1,2,0:T(8,128)(2,1)} collective-permute-done((bf16[1,64,10,2048]{3,1,2,0:T(8,128)(2,1)}, bf16[1,64,10,2048]{3,1,2,0:T(8,128)(2,1)}, u32[]{:S(2)}, u32[]{:S(2)}) %collective-permute-start.1) | collective-permute-done | bytes 2621472 | tf_op jit(solution)/shard_map/ppermute | solution.py:16
  192.7 0.3 collective-permute-start.3
  193.0 5.3 broadcast_in_dim.8
  198.4 2.9 copy_dynamic-update-slice_fusion
  201.3 3.6 bitcast_dynamic-update-slice_fusion.2
  204.9 0.0 collective-permute-done.2
  204.9 3.6 bitcast_dynamic-update-slice_fusion.1
  208.4 42.1 %collective-permute-done.3 = bf16[1,64,10,2048]{3,1,2,0:T(8,128)(2,1)} collective-permute-done((bf16[1,64,10,2048]{3,1,2,0:T(8,128)(2,1)}, bf16[1,64,10,2048]{3,1,2,0:T(8,128)(2,1)}, u32[]{:S(2)}, u32[]{:S(2)}) %collective-permute-start.3) | collective-permute-done | bytes 2621472 | tf_op jit(solution)/shard_map/ppermute | solution.py:16
  250.5 3.6 bitcast_dynamic-update-slice_fusion
  254.1 8.4 %fusion.14 = f32[2,256,5,256]{3,1,2,0:T(8,128)} fusion(bf16[256,2,5,2048]{3,0,2,1:T(8,128)(2,1)} %bitcast.83, bf16[2,2048,256]{2,1,0:T(8,128)(2,1)S(1)} %copy-done.12), kind=kOutput, calls=%fused_computation.25 | convolution fusion | flops 2684354560 | bytes 15204352 | tf_op jit(solution)/shard_map/nxcd,xdf->nxcf/dot_general | solution.py:113
  262.5 16.3 %convert_bitcast_fusion = bf16[256,2,5,2048]{3,0,2,1:T(8,128)(2,1)} fusion(bf16[2,256,2048]{2,1,0:T(8,128)(2,1)S(1)} %copy-done, f32[2,256,5,256]{3,1,2,0:T(8,128)} %fusion.14, bf16[256,2,5,2048]{3,0,2,1:T(8,128)(2,1)} %bitcast.84, bf16[2,2048,256]{2,1,0:T(8,128)(2,1)} %param.23), kind=kOutput, calls=%fused_computation.3 | convolution fusion | flops 5377884160 | bytes 27787264 | tf_op jit(solution)/shard_map/nxcf,xfd->nxcd/dot_general | solution.py:118
  278.8 15.3 %copy.47 = bf16[256,2,5,2048]{3,2,1,0:T(8,128)(2,1)} copy(bf16[256,2,5,2048]{3,0,2,1:T(8,128)(2,1)} %convert_bitcast_fusion) | data formatting | bytes 20971520 | tf_op jit(solution)/shard_map/convert_element_type | solution.py:120
  294.1 18.4 %convert_element_type.73 = bf16[2560,2048]{1,0:T(8,128)(2,1)} reshape(bf16[256,2,5,2048]{3,2,1,0:T(8,128)(2,1)} %copy.47) | data formatting | bytes 20971520 | tf_op jit(solution)/shard_map/convert_element_type | solution.py:120
  312.6 0.0 reduce-scatter.5.cloned.1.call-update
  312.6 0.9 copy-done.6
  313.5 2.1 collective-permute-start
  315.7 2.8 collective-permute-done
  318.5 0.1 fusion.37
  318.6 0.7 fusion.21
  319.3 0.1 broadcast_add_fusion
  319.4 0.2 copy.35
  319.6 90.7 %reduce-scatter.5.cloned.1.call-done = bf16[640,2048]{1,0:T(8,128)(2,1)} async-done(((bf16[2560,2048]{1,0:T(8,128)(2,1)}), bf16[640,2048]{1,0:T(8,128)(2,1)}) %reduce-scatter.5.cloned.1.call-update) | async-done | bytes 2621456 | tf_op jit(solution)/shard_map/reduce_scatter | solution.py:119
  410.4 5.4 reshape.114
  415.7 10.9 %all-to-all-start.1 = ((bf16[64,10,2048]{2,1,0:T(8,128)(2,1)}), bf16[64,10,2048]{2,1,0:T(8,128)(2,1)}, u32[]{:S(2)}, u32[]{:S(2)}) async-start(bf16[64,10,2048]{2,1,0:T(8,128)(2,1)} %reshape.114), calls=%async_computation.3 | async-start | bytes 8388608 | tf_op jit(solution)/shard_map/all_to_all | solution.py:127
  426.6 0.0 reduce-scatter.3.cloned.1.call-start
  426.7 0.0 copy-start.9
  426.7 2.3 convolution_convert_fusion
  429.0 0.0 reduce-scatter.3.cloned.1.call-update
  429.1 0.7 constant_dynamic-slice_fusion
  429.7 0.1 copy.48
  429.9 31.9 %reduce-scatter.3.cloned.1.call-done = bf16[128,2048]{1,0:T(8,128)(2,1)} async-done(((bf16[512,2048]{1,0:T(8,128)(2,1)}), bf16[128,2048]{1,0:T(8,128)(2,1)}) %reduce-scatter.3.cloned.1.call-update) | async-done | bytes 524304 | tf_op jit(solution)/shard_map/reduce_scatter | solution.py:103
  461.8 1.2 fusion.18
  463.0 2.0 fusion.20
  465.0 57.7 %all-to-all-done.1 = bf16[64,10,2048]{2,1,0:T(8,128)(2,1)} async-done(((bf16[64,10,2048]{2,1,0:T(8,128)(2,1)}), bf16[64,10,2048]{2,1,0:T(8,128)(2,1)}, u32[]{:S(2)}, u32[]{:S(2)}) %all-to-all-start.1) | async-done | bytes 2621472 | tf_op jit(solution)/shard_map/all_to_all | solution.py:127
  522.7 4.1 reshape.115
  526.8 3.3 gather_fusion.1
  530.1 5.4 reshape.116
  535.6 9.0 %multiply_reduce_fusion = f32[256,2048]{1,0:T(8,128)S(1)} fusion(f32[256,2,2048]{2,1,0:T(2,128)} %reshape.116, f32[256,2]{1,0:T(8,128)S(1)} %copy.48), kind=kLoop, calls=%fused_computation.4 | loop fusion | flops 1572864 | bytes 6293504 | tf_op jit(solution)/shard_map/reduce_sum | solution.py:132
  544.6 0.2 multiply_reduce_fusion.1
  544.9 1.2 multiply_convert_fusion
  (40 shorter events, 0.3 us)
Async XLA Ops:
  7.2 255.3 %copy-start = (bf16[2,256,2048]{2,1,0:T(8,128)(2,1)S(1)}, bf16[2,256,2048]{2,1,0:T(8,128)(2,1)}, u32[]{:S(2)}) copy-start(bf16[2,256,2048]{2,1,0:T(8,128)(2,1)} %param.24) | copy-start | bytes 6291460
  7.2 5.5 %copy-start.4 = (bf16[256,2048]{1,0:T(8,128)(2,1)S(1)}, bf16[256,2048]{1,0:T(8,128)(2,1)}, u32[]{:S(2)}) copy-start(bf16[256,2048]{1,0:T(8,128)(2,1)} %param.18) | copy-start | bytes 3145732
  7.2 5.8 %copy-start.8 = (f32[2048]{0:T(1024)S(1)}, f32[2048]{0:T(1024)}, u32[]{:S(2)}) copy-start(f32[2048]{0:T(1024)} %param.21) | copy-start | bytes 24580
  7.2 403.2 %reduce-scatter.5.cloned.1.call-start = ((), (), s32[]{:S(2)}) async-start(), calls=%async_computation.5 | async-start | bytes 13107200 | tf_op jit(solution)/shard_map/reduce_scatter | solution.py:119
  131.1 3.0 copy-start.2
  134.1 58.7 %collective-permute-start.1 = (bf16[1,64,10,2048]{3,1,2,0:T(8,128)(2,1)}, bf16[1,64,10,2048]{3,1,2,0:T(8,128)(2,1)}, u32[]{:S(2)}, u32[]{:S(2)}) collective-permute-start(bf16[1,64,10,2048]{3,1,2,0:T(8,128)(2,1)} %copy.42), channel_id=1, source_target_pairs={{0,1},{1,2},{2,3},{3,0},{4,5},{5,6},{6,7},{7,4},{8,9},{9,10},{10,1... | collective-permute-start | bytes 7864328 | tf_op jit(solution)/shard_map/ppermute | solution.py:16
  135.6 69.2 %collective-permute-start.2 = (bf16[1,64,10,2048]{3,1,2,0:T(8,128)(2,1)}, bf16[1,64,10,2048]{3,1,2,0:T(8,128)(2,1)}, u32[]{:S(2)}, u32[]{:S(2)}) collective-permute-start(bf16[1,64,10,2048]{3,1,2,0:T(8,128)(2,1)} %copy.42), channel_id=1, source_target_pairs={{0,3},{1,0},{2,1},{3,2},{4,7},{5,4},{6,5},{7,6},{8,11},{9,8},{10,9... | collective-permute-start | bytes 7864328 | tf_op jit(solution)/shard_map/ppermute | solution.py:19
  192.7 57.8 %collective-permute-start.3 = (bf16[1,64,10,2048]{3,1,2,0:T(8,128)(2,1)}, bf16[1,64,10,2048]{3,1,2,0:T(8,128)(2,1)}, u32[]{:S(2)}, u32[]{:S(2)}) collective-permute-start(bf16[1,64,10,2048]{3,1,2,0:T(8,128)(2,1)} %collective-permute-done.1), channel_id=1, source_target_pairs={{0,1},{1,2},{2,3},{3,0},{4,5},{5,6},{6,7},{7,4},{8,9},{9,10},{10,1... | collective-permute-start | bytes 7864328 | tf_op jit(solution)/shard_map/ppermute | solution.py:16
  193.0 5.3 copy-start.3
  208.4 45.7 %copy-start.12 = (bf16[2,2048,256]{2,1,0:T(8,128)(2,1)S(1)}, bf16[2,2048,256]{2,1,0:T(8,128)(2,1)}, u32[]{:S(2)}) copy-start(bf16[2,2048,256]{2,1,0:T(8,128)(2,1)} %param.22) | copy-start | bytes 6291460
  312.6 0.9 copy-start.6
  313.5 5.0 collective-permute-start
  415.7 11.0 %copy-start.5 = (bf16[256,2048]{1,0:T(8,128)(2,1)S(1)}, bf16[256,2048]{1,0:T(8,128)(2,1)}, u32[]{:S(2)}) copy-start(bf16[256,2048]{1,0:T(8,128)(2,1)} %param.16) | copy-start | bytes 3145732
  415.7 11.0 %copy-start.7 = (bf16[1,256,256]{2,1,0:T(8,128)(2,1)S(1)}, bf16[1,256,256]{2,1,0:T(8,128)(2,1)}, u32[]{:S(2)}) copy-start(bf16[1,256,256]{2,1,0:T(8,128)(2,1)} %param.14) | copy-start | bytes 393220
  415.7 11.0 %copy-start.11 = (f32[256]{0:T(256)S(1)}, f32[256]{0:T(256)}, u32[]{:S(2)}) copy-start(f32[256]{0:T(256)} %param.15) | copy-start | bytes 3076
  415.7 107.0 %all-to-all-start.1 = ((bf16[64,10,2048]{2,1,0:T(8,128)(2,1)}), bf16[64,10,2048]{2,1,0:T(8,128)(2,1)}, u32[]{:S(2)}, u32[]{:S(2)}) async-start(bf16[64,10,2048]{2,1,0:T(8,128)(2,1)} %reshape.114), calls=%async_computation.3 | async-start | bytes 8388608 | tf_op jit(solution)/shard_map/all_to_all | solution.py:127
  426.6 35.1 %reduce-scatter.3.cloned.1.call-start = ((), (), s32[]{:S(2)}) async-start(), calls=%async_computation.4 | async-start | bytes 2621440 | tf_op jit(solution)/shard_map/reduce_scatter | solution.py:103
  426.7 36.3 %copy-start.9 = (f32[2048]{0:T(1024)S(1)}, f32[2048]{0:T(1024)}, u32[]{:S(2)}) copy-start(f32[2048]{0:T(1024)} %param.17) | copy-start | bytes 24580
  535.6 9.3 %copy-start.10 = (f32[2048]{0:T(1024)S(1)}, f32[2048]{0:T(1024)}, u32[]{:S(2)}) copy-start(f32[2048]{0:T(1024)} %param.25) | copy-start | bytes 24580
  535.6 10.5 %copy-start.1 = (bf16[2,256,2048]{2,1,0:T(8,128)(2,1)S(1)}, bf16[2,256,2048]{2,1,0:T(8,128)(2,1)}, u32[]{:S(2)}) copy-start(bf16[2,256,2048]{2,1,0:T(8,128)(2,1)} %param.24) | copy-start | bytes 6291460
Sparse Core Ops, SparseCore 0:
  312.7 97.6 reduce-scatter.4
  430.0 31.7 reduce-scatter.2
